TPU v7x, 512 devices: a whole 4x4x16 slice. The times are simulated.
512 devices in a mesh: ep: 32 (over z, core), tp: 16 (over y, x).
Axes of the slice: x: 4, y: 4, z: 16, core: 2. Of those that a mesh axis runs over, the one named last changes fastest.
Arguments:
- mixer_input_channels: bfloat16 [8192, 4096], P('ep', 'tp'), may hold values from -6 to 6
- input_state_projection: bfloat16 [8192, 4096], P('ep', 'tp'), may hold values from -6 to 6
- output_state_projection: bfloat16 [8192, 4096], P('ep', 'tp'), may hold values from -6 to 6
- output_gate_logits: bfloat16 [8192, 4096], P('ep', 'tp'), may hold values from -6 to 6
- step_size_logits: float32 [8192, 64], P('ep', 'tp'), may hold values from -4.4 to 2.9
- extra_log_decay: float32 [8192, 64], P('ep', 'tp'), may hold values from -2.1 to 0, as said below
- mixer_channel_taps: bfloat16 [4, 4096], P(None, 'tp'), may hold values from -3 to 3
- input_state_taps: bfloat16 [4, 4096], P(None, 'tp'), may hold values from -3 to 3
- output_state_taps: bfloat16 [4, 4096], P(None, 'tp'), may hold values from -3 to 3
- decay_rate_log: float32 [64], P('tp')
- head_skip_weight: float32 [64], P('tp'), may hold values from 0.1 to 1.9
- grouped_norm_gain: float32 [4096], P('tp'), may hold values from 0.1 to 1.9
- mixer_output_weight: bfloat16 [4096, 2048], P('tp'), may hold values from -0.09375 to 0.09375
- expert_input_tokens: bfloat16 [4096, 2048], P('ep'), may hold values from -6 to 6
- routing: int32 [4096, 2], P('ep'), may hold values from 0 to 31, all different within a row; in each aligned block of 128 rows (0 to 127, 128 to 255, ...) at most 10 rows name the same one
- router_chosen_scores: float32 [4096, 2], P('ep'), may hold values from 0.05 to 1
- expert_norm_gain: float32 [2048], replicated, may hold values from 0.1 to 1.9
- expert_gate_weight: bfloat16 [32, 2048, 2048], P('ep', None, 'tp'), may hold values from -0.125 to 0.125
- expert_up_weight: bfloat16 [32, 2048, 2048], P('ep', None, 'tp'), may hold values from -0.125 to 0.125
- expert_down_weight: bfloat16 [32, 2048, 2048], P('ep', 'tp'), may hold values from -0.125 to 0.125
Outputs:
- mixer_output_first: bfloat16 [8192, 2048], P('ep', 'tp')
- moe_out: bfloat16 [4096, 2048], P('ep', 'tp')
Inputs may be any that keep to these rules, and one draw needn't show every extreme that they name: `routing`: within the rows of one index of ep (aligned blocks of 128 rows) no expert is named more than 10 times, some expert exactly 10 times; a row names 2 different experts. `extra_log_decay`: zero at all but a few positions.
All inputs are finite; a program needn't handle non-finite values.
Results may differ from a plain program's by a relative error of at most 0.018.
Values may be sent and summed in bfloat16 or wider, within the bound.
No kernel may reach another device: no remote copies, remote signals or barrier semaphores. Data moves between devices by JAX's collectives and lax.ppermute only.
A program may use at most 64 MiB of HBM per device.

v0:
```python
import jax
import jax.numpy as jnp
from jax import lax
from jax.sharding import Mesh
from jax.sharding import PartitionSpec as P

HEAD_DIM = 64
STATE = 128
BLOCK = 128
EP = ("ep_0", "ep_1")


eps = 1e-06


def passed_along(block, axis, distance):
    devices = range(lax.axis_size(axis))
    route = [(i - distance, i) for i in devices if i - distance in devices]
    return lax.ppermute(block, axis, route)


def neutral_like(value, identity):
    return jax.tree.map(
        lambda a, e: jnp.broadcast_to(jnp.asarray(e, a.dtype), a.shape), value, identity
    )


def entering_2(value, axes, combine, identity):
    before = start = neutral_like(value, identity)
    running = value
    for axis in reversed(axes):
        peers, index = (lax.axis_size(axis), lax.axis_index(axis))
        pieces = jax.tree.map(
            lambda part, kind: lax.all_gather(part.astype(kind), axis),
            running,
            (jnp.bfloat16, jnp.bfloat16),
        )
        inside, running = (start, start)
        for k in range(peers):
            passed = k < index
            running = combine(
                running, jax.tree.map(lambda part, own: part[k].astype(own.dtype), pieces, value)
            )
            inside = jax.tree.map(lambda new, old: jnp.where(passed, new, old), running, inside)
        before = combine(inside, before)
    return before


def copy_for_each(value, axis):
    copies = jnp.broadcast_to(value, (lax.axis_size(axis), *value.shape))
    return lax.all_to_all(copies, axis, split_axis=0, concat_axis=0, tiled=True)


def in_order(parts, dim):
    parts = jnp.moveaxis(parts, 0, dim)
    lengths = parts.shape
    return parts.reshape(*lengths[:dim], lengths[dim] * lengths[dim + 1], *lengths[dim + 2 :])


def gather_directly(value, axis, dim):
    parts = copy_for_each(value, axis)
    return in_order(parts, dim)


def split_up(value, dim, peers):
    before, after = (value.shape[:dim], value.shape[dim + 1 :])
    return jnp.moveaxis(value.reshape(*before, peers, -1, *after), dim, 0)


def sent_and_summed(value, axis, dim):
    parts = split_up(value, dim, lax.axis_size(axis))
    arrived = lax.all_to_all(parts, axis, split_axis=0, concat_axis=0, tiled=True)
    return arrived.astype(jnp.float32).sum(axis=0)


def conv_silu(prior, values, taps):
    length = values.shape[0]
    padded = jnp.concatenate([prior, values], axis=0).astype(jnp.float32)
    total = jnp.zeros(values.shape, jnp.float32)
    for index in range(taps.shape[0]):
        total = total + padded[index : index + length] * taps[index].astype(jnp.float32)
    return jax.nn.silu(total).astype(jnp.bfloat16)


def join_states(earlier, later):
    return (earlier[0] * later[0], earlier[1] * later[0][:, None, None] + later[1])


def mixer_terms(
    mixer_input_channels,
    input_state_projection,
    output_state_projection,
    output_gate_logits,
    step_size_logits,
    extra_log_decay,
    mixer_channel_taps,
    input_state_taps,
    output_state_taps,
    decay_rate_log,
    head_skip_weight,
    grouped_norm_gain,
    mixer_output_weight,
):
    length = mixer_input_channels.shape[0]
    heads = decay_rate_log.shape[0]
    groups = input_state_projection.shape[1] // STATE
    per_group = heads // groups
    blocks = length // BLOCK
    reach = mixer_channel_taps.shape[0] - 1
    prior = passed_along(
        (
            mixer_input_channels[length - reach :],
            input_state_projection[length - reach :],
            output_state_projection[length - reach :],
        ),
        EP,
        1,
    )
    x_conv = conv_silu(prior[0], mixer_input_channels, mixer_channel_taps)
    b_conv = conv_silu(prior[1], input_state_projection, input_state_taps)
    c_conv = conv_silu(prior[2], output_state_projection, output_state_taps)
    step_size = jax.nn.softplus(step_size_logits)
    head_log_decay = step_size * -jnp.exp(decay_rate_log) + extra_log_decay
    decay_sum = jnp.cumsum(head_log_decay.reshape(blocks, BLOCK, heads), axis=1)
    x_blocks = x_conv.reshape(blocks, BLOCK, heads, HEAD_DIM)
    x_step = (
        x_blocks.astype(jnp.float32) * step_size.reshape(blocks, BLOCK, heads)[..., None]
    ).astype(jnp.bfloat16)
    b_blocks = b_conv.reshape(blocks, BLOCK, groups, STATE)
    c_blocks = c_conv.reshape(blocks, BLOCK, groups, STATE)
    inner = jnp.einsum("blgn,bsgn->bgls", c_blocks, b_blocks, preferred_element_type=jnp.float32)
    across = jnp.transpose(decay_sum, (0, 2, 1)).reshape(blocks, groups, per_group, BLOCK)
    order = jnp.arange(BLOCK, dtype=jnp.int32)
    causal = order[:, None] >= order[None, :]
    distance = across[..., :, None] - across[..., None, :]
    decay = jnp.where(causal, jnp.exp(jnp.where(causal, distance, 0.0)), 0.0)
    scores = (inner[:, :, None] * decay).astype(jnp.bfloat16).reshape(blocks, heads, BLOCK, BLOCK)
    y_diag = jnp.einsum("bhls,bshp->blhp", scores, x_step, preferred_element_type=jnp.float32)
    block_last = decay_sum[:, -1]
    x_weighted = (
        x_step.astype(jnp.float32) * jnp.exp(block_last[:, None, :] - decay_sum)[..., None]
    ).astype(jnp.bfloat16)
    states = jnp.einsum(
        "blgn,blgep->bgepn",
        b_blocks,
        x_weighted.reshape(blocks, BLOCK, groups, per_group, HEAD_DIM),
        preferred_element_type=jnp.float32,
    ).reshape(blocks, heads, HEAD_DIM, STATE)

    def carry_step(state, inputs):
        return (state * inputs[1][:, None, None] + inputs[0], state)

    total, before = lax.scan(
        carry_step, jnp.zeros((heads, HEAD_DIM, STATE), jnp.float32), (states, jnp.exp(block_last))
    )
    device_decay = jnp.exp(jnp.sum(block_last, axis=0))
    incoming = entering_2(
        (device_decay, total), EP, join_states, (jnp.ones_like(device_decay), jnp.zeros_like(total))
    )
    entry = jnp.cumsum(block_last, axis=0) - block_last
    entering = (before + incoming[1][None] * jnp.exp(entry)[:, :, None, None]).astype(jnp.bfloat16)
    y_off = jnp.einsum(
        "blgn,bgepn->blgep",
        c_blocks,
        entering.reshape(blocks, groups, per_group, HEAD_DIM, STATE),
        preferred_element_type=jnp.float32,
    ).reshape(blocks, BLOCK, heads, HEAD_DIM)
    y_off = y_off * jnp.exp(decay_sum)[..., None]
    mixed = (y_diag + y_off + head_skip_weight[:, None] * x_blocks.astype(jnp.float32)).reshape(
        length, heads * HEAD_DIM
    )
    mixed = mixed * jax.nn.silu(output_gate_logits.astype(jnp.float32))
    grouped = mixed.reshape(length, groups, per_group * HEAD_DIM)
    grouped = grouped * lax.rsqrt(jnp.mean(grouped * grouped, axis=-1, keepdims=True) + eps)
    mix_normed = (grouped.reshape(length, heads * HEAD_DIM) * grouped_norm_gain).astype(
        jnp.bfloat16
    )
    return jnp.dot(mix_normed, mixer_output_weight, preferred_element_type=jnp.float32)


def expert_terms(
    expert_input_tokens,
    routing,
    expert_norm_gain,
    expert_gate_weight,
    expert_up_weight,
    expert_down_weight,
):
    parts = lax.axis_size("tp")
    devices = lax.axis_size(EP)
    local_experts = expert_gate_weight.shape[0]
    experts = local_experts * devices
    tokens = expert_input_tokens.shape[0]
    top_count = routing.shape[1]
    model = expert_input_tokens.shape[1]
    columns = model // parts
    capacity = (tokens * top_count * 5 + 4 * experts - 1) // (4 * experts)
    rows = expert_input_tokens.astype(jnp.float32)
    normed = (
        rows * lax.rsqrt(jnp.mean(rows * rows, axis=-1, keepdims=True) + eps) * expert_norm_gain
    ).astype(jnp.bfloat16)
    flat = routing.reshape(tokens * top_count)
    member = (flat[:, None] == jnp.arange(experts, dtype=jnp.int32)[None, :]).astype(jnp.int32)
    rank = jnp.sum((jnp.cumsum(member, axis=0) - member) * member, axis=1)
    slot = flat * capacity + rank
    pick = (slot[:, None] == jnp.arange(experts * capacity, dtype=jnp.int32)[None, :]).astype(
        jnp.bfloat16
    )
    pick = pick.reshape(tokens, top_count, experts * capacity)
    own = lax.dynamic_slice_in_dim(normed, lax.axis_index("tp") * columns, columns, 1)
    outgoing = jnp.einsum("tks,tc->sc", pick, own, preferred_element_type=jnp.float32).astype(
        jnp.bfloat16
    )
    arrived = lax.all_to_all(
        outgoing.reshape(experts, capacity, columns), EP, split_axis=0, concat_axis=0, tiled=True
    )
    arranged = jnp.moveaxis(arrived.reshape(devices, local_experts, capacity, columns), 1, 0)
    arranged = arranged.reshape(local_experts, devices * capacity, columns)
    piece = gather_directly(arranged, "tp", 2)
    gate = jnp.einsum("erc,ecf->erf", piece, expert_gate_weight, preferred_element_type=jnp.float32)
    up = jnp.einsum("erc,ecf->erf", piece, expert_up_weight, preferred_element_type=jnp.float32)
    hidden = (jax.nn.silu(gate) * up).astype(jnp.bfloat16)
    partial_value = jnp.einsum(
        "erf,efd->erd", hidden, expert_down_weight, preferred_element_type=jnp.float32
    )
    return (partial_value.reshape(local_experts * devices * capacity, model), pick)


def expert_return(summed, pick, router_chosen_scores, local_experts):
    devices = lax.axis_size(EP)
    columns = summed.shape[1]
    capacity = summed.shape[0] // (local_experts * devices)
    back = jnp.moveaxis(summed.reshape(local_experts, devices, capacity, columns), 0, 1)
    back = back.reshape(devices * local_experts, capacity, columns)
    returned = lax.all_to_all(back, EP, split_axis=0, concat_axis=0, tiled=True)
    table = returned.reshape(devices * local_experts * capacity, columns)
    share = router_chosen_scores / jnp.sum(router_chosen_scores, axis=1, keepdims=True)
    total = jnp.zeros((pick.shape[0], columns), jnp.float32)
    for index in range(pick.shape[1]):
        total = total + share[:, index : index + 1] * jnp.dot(
            pick[:, index], table, preferred_element_type=jnp.float32
        )
    return total.astype(jnp.bfloat16)


def per_device(
    mixer_input_channels,
    input_state_projection,
    output_state_projection,
    output_gate_logits,
    step_size_logits,
    extra_log_decay,
    mixer_channel_taps,
    input_state_taps,
    output_state_taps,
    decay_rate_log,
    head_skip_weight,
    grouped_norm_gain,
    mixer_output_weight,
    expert_input_tokens,
    routing,
    router_chosen_scores,
    expert_norm_gain,
    expert_gate_weight,
    expert_up_weight,
    expert_down_weight,
):
    mixer_part = mixer_terms(
        mixer_input_channels,
        input_state_projection,
        output_state_projection,
        output_gate_logits,
        step_size_logits,
        extra_log_decay,
        mixer_channel_taps,
        input_state_taps,
        output_state_taps,
        decay_rate_log,
        head_skip_weight,
        grouped_norm_gain,
        mixer_output_weight,
    )
    expert_part, pick = expert_terms(
        expert_input_tokens,
        routing,
        expert_norm_gain,
        expert_gate_weight,
        expert_up_weight,
        expert_down_weight,
    )
    mixer_sum = sent_and_summed(mixer_part.astype(jnp.bfloat16), "tp", 1)
    expert_sum = sent_and_summed(expert_part.astype(jnp.bfloat16), "tp", 1)
    mixer_output_first = mixer_sum.astype(jnp.bfloat16)
    moe_out = expert_return(
        expert_sum.astype(jnp.bfloat16), pick, router_chosen_scores, expert_gate_weight.shape[0]
    )
    return (mixer_output_first, moe_out)


def solution(mesh):
    split = Mesh(mesh.devices.reshape(16, 2, mesh.shape["tp"]), ("ep_0", "ep_1", "tp"))
    in_specs = (
        P(EP, "tp"),
        P(EP, "tp"),
        P(EP, "tp"),
        P(EP, "tp"),
        P(EP, "tp"),
        P(EP, "tp"),
        P(None, "tp"),
        P(None, "tp"),
        P(None, "tp"),
        P("tp"),
        P("tp"),
        P("tp"),
        P("tp", None),
        P(EP, None),
        P(EP, None),
        P(EP, None),
        P(),
        P(EP, None, "tp"),
        P(EP, None, "tp"),
        P(EP, "tp", None),
    )
    out_specs = (P(EP, "tp"), P(EP, "tp"))
    return jax.shard_map(
        per_device, mesh=split, in_specs=in_specs, out_specs=out_specs, check_vma=False
    )
```

profile of v0, /device:TPU:1, one launch (start us, length us, event | category | flops | bytes accessed | tf_op | source)
XLA Modules:
  0.0 210.5 jit_solution(14468817215203457189)
XLA Ops:
  8.1 4.9 %collective-permute-start = (bf16[3,256]{0,1:T(8,128)(2,1)S(1)}, bf16[3,256]{0,1:T(8,128)(2,1)S(1)}, u32[]{:S(2)}, u32[]{:S(2)}) collective-permute-start(bf16[3,256]{0,1:T(8,128)(2,1)S(1)} %copy.94), channel_id=1, source_target_pairs={{0,16},{16,32},{32,48},{48,64},{64,80},{80,96},{96,112},{112,128},... | collective-permute-start | bytes 4616 | tf_op jit(solution)/shard_map/ppermute | solution.py:19
  13.9 1.9 collective-permute-start.2
  17.3 4.0 %collective-permute-start.1 = (bf16[3,256]{0,1:T(8,128)(2,1)}, bf16[3,256]{0,1:T(8,128)(2,1)}, u32[]{:S(2)}, u32[]{:S(2)}) collective-permute-start(bf16[3,256]{0,1:T(8,128)(2,1)} %copy.96), channel_id=1, source_target_pairs={{0,16},{16,32},{32,48},{48,64},{64,80},{80,96},{96,112},{112,128},... | collective-permute-start | bytes 4616 | tf_op jit(solution)/shard_map/ppermute | solution.py:19
  22.5 1.1 convert_element_type.498
  26.8 13.6 %all-to-all-start.1 = ((bf16[32,10,128]{2,1,0:T(8,128)(2,1)}), bf16[32,10,128]{2,1,0:T(8,128)(2,1)S(1)}, u32[]{:S(2)}, u32[]{:S(2)}) async-start(bf16[32,10,128]{2,1,0:T(8,128)(2,1)} %reshape.340), calls=%async_computation.1 | async-start | bytes 262144 | tf_op jit(solution)/shard_map/all_to_all | solution.py:214
  41.6 1.3 dynamic-slice
  43.9 2.5 %all-reduce = bf16[8]{0:T(256)(128)(2,1)S(1)} all-reduce(bf16[8]{0:T(256)(128)(2,1)S(1)} %dynamic-update-slice), channel_id=2, replica_groups=mesh['ep_0'=16,'ep_1'=2,'tp'=16] {'ep_1'}, use_global_device_ids=true, to_apply=%add | all-reduce | flops 8 | bytes 32
  49.4 22.2 %all-gather.2 = bf16[16,1,4]{2,1,0:T(2,128)(2,1)S(1)} all-gather(bf16[1,1,4]{2,1,0:T(2,128)(2,1)S(1)} %get-tuple-element.96), channel_id=1, replica_groups=mesh['ep_0'=16,'ep_1'=2,'tp'=16] {'ep_0'}, dimensions={0}, use_global_device_ids=true | all-gather | bytes 136 | tf_op jit(solution)/shard_map/all_gather | solution.py:34
  73.9 9.1 %all-gather.1 = bf16[8,64,128]{2,1,0:T(8,128)(2,1)S(1)} all-gather(bf16[4,64,128]{2,1,0:T(8,128)(2,1)S(1)} %convert_element_type.438), channel_id=3, replica_groups=mesh['ep_0'=16,'ep_1'=2,'tp'=16] {'ep_1'}, dimensions={0}, use_global_device_ids=true | all-gather | bytes 196608 | tf_op jit(solution)/shard_map/all_gather | solution.py:34
  83.8 1.3 broadcast_in_dim.22
  85.2 6.9 %all-to-all-start.2 = ((bf16[16,1,320,128]{3,2,1,0:T(8,128)(2,1)}), bf16[16,1,320,128]{3,2,1,0:T(8,128)(2,1)S(1)}, u32[]{:S(2)}, u32[]{:S(2)}) async-start(bf16[16,1,320,128]{3,2,1,0:T(8,128)(2,1)} %broadcast_in_dim.22), calls=%async_computation.2 | async-start | bytes 2621440 | tf_op jit(solution)/shard_map/all_to_all | solution.py:51
  95.4 1.3 copy.129
  97.9 1.8 multiply_convert_fusion.5
  100.7 1.4 multiply_convert_fusion.6
  103.0 9.3 %all-to-all-done.2 = bf16[16,1,320,128]{3,2,1,0:T(8,128)(2,1)S(1)} async-done(((bf16[16,1,320,128]{3,2,1,0:T(8,128)(2,1)}), bf16[16,1,320,128]{3,2,1,0:T(8,128)(2,1)S(1)}, u32[]{:S(2)}, u32[]{:S(2)}) %all-to-all-start.2) | async-done | bytes 1310752 | tf_op jit(solution)/shard_map/all_to_all | solution.py:51
  114.8 3.9 %fusion.1 = bf16[16,320,128]{2,1,0:T(8,128)(2,1)} fusion(bf16[16,128,128]{2,1,0:T(8,128)(2,1)S(1)} %bitcast.254, bf16[40,8,16,128]{3,2,1,0:T(8,128)(2,1)} %bitcast.247, bf16[1,2048,128]{2,1,0:T(8,128)(2,1)S(1)} %copy-done.8, f32[320,128]{1,0:T(8,128)S(1)} %fusion.5), kind=kOutput, calls=%fused_computation.6 | convolution fusion | flops 336445440 | bytes 3833856 | tf_op jit(solution)/shard_map/erf,efd->erd/dot_general | solution.py:223
  118.9 4.2 %all-to-all-start.3 = ((bf16[16,320,128]{2,1,0:T(8,128)(2,1)}), bf16[16,320,128]{2,1,0:T(8,128)(2,1)S(1)}, u32[]{:S(2)}, u32[]{:S(2)}) async-start(bf16[16,320,128]{2,1,0:T(8,128)(2,1)} %fusion.1), calls=%async_computation.3 | async-start | bytes 2621440 | tf_op jit(solution)/shard_map/all_to_all | solution.py:72
  123.1 19.8 %all-gather.5.cloned.1.call-done = bf16[16,4,64,128]{3,2,1,0:T(8,128)(2,1)} async-done(((bf16[1,4,64,128]{3,2,1,0:T(8,128)(2,1)}), bf16[16,4,64,128]{3,2,1,0:T(8,128)(2,1)}) %all-gather.5.cloned.1.call-update) | async-done | bytes 1048592 | tf_op jit(solution)/shard_map/all_gather | solution.py:34
  143.2 1.7 fusion.55
  146.8 1.3 copy.172
  148.1 6.4 %all-to-all-start = ((bf16[16,256,128]{2,1,0:T(8,128)(2,1)}), bf16[16,256,128]{2,1,0:T(8,128)(2,1)S(1)}, u32[]{:S(2)}, u32[]{:S(2)}) async-start(bf16[16,256,128]{2,1,0:T(8,128)(2,1)} %bitcast.248), calls=%async_computation | async-start | bytes 2097152 | tf_op jit(solution)/shard_map/all_to_all | solution.py:72
  155.4 11.3 %all-to-all-done = bf16[16,256,128]{2,1,0:T(8,128)(2,1)S(1)} async-done(((bf16[16,256,128]{2,1,0:T(8,128)(2,1)}), bf16[16,256,128]{2,1,0:T(8,128)(2,1)S(1)}, u32[]{:S(2)}, u32[]{:S(2)}) %all-to-all-start) | async-done | bytes 1048608 | tf_op jit(solution)/shard_map/all_to_all | solution.py:72
  166.7 19.9 %all-to-all-start.4 = ((bf16[32,10,128]{2,1,0:T(8,128)(2,1)}), bf16[32,10,128]{2,1,0:T(8,128)(2,1)S(1)}, u32[]{:S(2)}, u32[]{:S(2)}) async-start(bf16[32,10,128]{2,1,0:T(8,128)(2,1)} %reshape_transpose_reshape.7), calls=%async_computation.4 | async-start | bytes 262144 | tf_op jit(solution)/shard_map/all_to_all | solution.py:235
  187.5 15.0 %all-to-all-done.4 = bf16[32,10,128]{2,1,0:T(8,128)(2,1)S(1)} async-done(((bf16[32,10,128]{2,1,0:T(8,128)(2,1)}), bf16[32,10,128]{2,1,0:T(8,128)(2,1)S(1)}, u32[]{:S(2)}, u32[]{:S(2)}) %all-to-all-start.4) | async-done | bytes 81952 | tf_op jit(solution)/shard_map/all_to_all | solution.py:235
  (211 shorter events, 28.7 us)
Async XLA Ops:
  7.2 139.2 %copy-start = (bf16[256,2048]{1,0:T(8,128)(2,1)S(1)}, bf16[256,2048]{1,0:T(8,128)(2,1)}, u32[]{:S(2)}) copy-start(bf16[256,2048]{1,0:T(8,128)(2,1)} %param.34) | copy-start | bytes 3145732
  8.1 63.5 %collective-permute-start = (bf16[3,256]{0,1:T(8,128)(2,1)S(1)}, bf16[3,256]{0,1:T(8,128)(2,1)S(1)}, u32[]{:S(2)}, u32[]{:S(2)}) collective-permute-start(bf16[3,256]{0,1:T(8,128)(2,1)S(1)} %copy.94), channel_id=1, source_target_pairs={{0,16},{16,32},{32,48},{48,64},{64,80},{80,96},{96,112},{112,128},... | collective-permute-start | bytes 4616 | tf_op jit(solution)/shard_map/ppermute | solution.py:19
  13.9 58.4 %collective-permute-start.2 = (bf16[3,256]{0,1:T(8,128)(2,1)S(1)}, bf16[3,256]{0,1:T(8,128)(2,1)S(1)}, u32[]{:S(2)}, u32[]{:S(2)}) collective-permute-start(bf16[3,256]{0,1:T(8,128)(2,1)S(1)} %copy.98), channel_id=1, source_target_pairs={{0,16},{16,32},{32,48},{48,64},{64,80},{80,96},{96,112},{112,128},... | collective-permute-start | bytes 4616 | tf_op jit(solution)/shard_map/ppermute | solution.py:19
  17.3 79.6 %collective-permute-start.1 = (bf16[3,256]{0,1:T(8,128)(2,1)}, bf16[3,256]{0,1:T(8,128)(2,1)}, u32[]{:S(2)}, u32[]{:S(2)}) collective-permute-start(bf16[3,256]{0,1:T(8,128)(2,1)} %copy.96), channel_id=1, source_target_pairs={{0,16},{16,32},{32,48},{48,64},{64,80},{80,96},{96,112},{112,128},... | collective-permute-start | bytes 4616 | tf_op jit(solution)/shard_map/ppermute | solution.py:19
  23.7 24.3 %copy-start.13 = (bf16[256,256]{1,0:T(8,128)(2,1)S(1)}, bf16[256,256]{1,0:T(8,128)(2,1)}, u32[]{:S(2)}) copy-start(bf16[256,256]{1,0:T(8,128)(2,1)} %param.24) | copy-start | bytes 393220
  26.8 57.0 %all-to-all-start.1 = ((bf16[32,10,128]{2,1,0:T(8,128)(2,1)}), bf16[32,10,128]{2,1,0:T(8,128)(2,1)S(1)}, u32[]{:S(2)}, u32[]{:S(2)}) async-start(bf16[32,10,128]{2,1,0:T(8,128)(2,1)} %reshape.340), calls=%async_computation.1 | async-start | bytes 262144 | tf_op jit(solution)/shard_map/all_to_all | solution.py:214
  40.4 102.6 %all-gather.5.cloned.1.call-start = ((), (), s32[]{:S(2)}) async-start(), calls=%async_computation.5 | async-start | bytes 1114112 | tf_op jit(solution)/shard_map/all_gather | solution.py:34
  46.4 36.6 %copy-start.29 = (f32[4]{0:T(128)}, f32[4]{0:T(128)S(1)}, u32[]{:S(2)}) copy-start(f32[4]{0:T(128)S(1)} %slice_convert_fusion.13) | copy-start | bytes 52
  47.7 35.3 %copy-start.22 = (f32[4]{0:T(128)}, f32[4]{0:T(128)S(1)}, u32[]{:S(2)}) copy-start(f32[4]{0:T(128)S(1)} %get-tuple-element.97) | copy-start | bytes 52
  85.2 27.2 %all-to-all-start.2 = ((bf16[16,1,320,128]{3,2,1,0:T(8,128)(2,1)}), bf16[16,1,320,128]{3,2,1,0:T(8,128)(2,1)S(1)}, u32[]{:S(2)}, u32[]{:S(2)}) async-start(bf16[16,1,320,128]{3,2,1,0:T(8,128)(2,1)} %broadcast_in_dim.22), calls=%async_computation.2 | async-start | bytes 2621440 | tf_op jit(solution)/shard_map/all_to_all | solution.py:51
  118.7 24.2 %copy-start.33 = (f32[4]{0:T(128)S(1)}, f32[4]{0:T(128)}, u32[]{:S(2)}) copy-start(f32[4]{0:T(128)} %get-tuple-element.64) | copy-start | bytes 52
  118.7 24.2 %copy-start.34 = (f32[4]{0:T(128)S(1)}, f32[4]{0:T(128)}, u32[]{:S(2)}) copy-start(f32[4]{0:T(128)} %get-tuple-element.65) | copy-start | bytes 52
  118.8 24.2 %copy-start.35 = (f32[4]{0:T(128)S(1)}, f32[4]{0:T(128)}, u32[]{:S(2)}) copy-start(f32[4]{0:T(128)} %get-tuple-element.66) | copy-start | bytes 52
  118.8 24.2 %copy-start.36 = (f32[4]{0:T(128)S(1)}, f32[4]{0:T(128)}, u32[]{:S(2)}) copy-start(f32[4]{0:T(128)} %get-tuple-element.67) | copy-start | bytes 52
  118.8 24.2 %copy-start.37 = (f32[4]{0:T(128)S(1)}, f32[4]{0:T(128)}, u32[]{:S(2)}) copy-start(f32[4]{0:T(128)} %get-tuple-element.68) | copy-start | bytes 52
  118.8 24.2 %copy-start.38 = (f32[4]{0:T(128)S(1)}, f32[4]{0:T(128)}, u32[]{:S(2)}) copy-start(f32[4]{0:T(128)} %get-tuple-element.69) | copy-start | bytes 52
  118.8 24.2 %copy-start.39 = (f32[4]{0:T(128)S(1)}, f32[4]{0:T(128)}, u32[]{:S(2)}) copy-start(f32[4]{0:T(128)} %get-tuple-element.70) | copy-start | bytes 52
  118.8 24.2 %copy-start.40 = (f32[4]{0:T(128)S(1)}, f32[4]{0:T(128)}, u32[]{:S(2)}) copy-start(f32[4]{0:T(128)} %get-tuple-element.71) | copy-start | bytes 52
  118.8 24.2 %copy-start.41 = (f32[4]{0:T(128)S(1)}, f32[4]{0:T(128)}, u32[]{:S(2)}) copy-start(f32[4]{0:T(128)} %get-tuple-element.72) | copy-start | bytes 52
  118.8 24.2 %copy-start.42 = (f32[4]{0:T(128)S(1)}, f32[4]{0:T(128)}, u32[]{:S(2)}) copy-start(f32[4]{0:T(128)} %get-tuple-element.73) | copy-start | bytes 52
  118.9 29.2 %all-to-all-start.3 = ((bf16[16,320,128]{2,1,0:T(8,128)(2,1)}), bf16[16,320,128]{2,1,0:T(8,128)(2,1)S(1)}, u32[]{:S(2)}, u32[]{:S(2)}) async-start(bf16[16,320,128]{2,1,0:T(8,128)(2,1)} %fusion.1), calls=%async_computation.3 | async-start | bytes 2621440 | tf_op jit(solution)/shard_map/all_to_all | solution.py:72
  148.1 18.6 %all-to-all-start = ((bf16[16,256,128]{2,1,0:T(8,128)(2,1)}), bf16[16,256,128]{2,1,0:T(8,128)(2,1)S(1)}, u32[]{:S(2)}, u32[]{:S(2)}) async-start(bf16[16,256,128]{2,1,0:T(8,128)(2,1)} %bitcast.248), calls=%async_computation | async-start | bytes 2097152 | tf_op jit(solution)/shard_map/all_to_all | solution.py:72
  154.5 32.1 %copy-start.18 = (s32[128,2]{0,1:T(2,128)S(1)}, s32[128,2]{0,1:T(2,128)}, u32[]{:S(2)}) copy-start(s32[128,2]{0,1:T(2,128)} %copy-done.17) | copy-start | bytes 3076
  166.7 35.7 %all-to-all-start.4 = ((bf16[32,10,128]{2,1,0:T(8,128)(2,1)}), bf16[32,10,128]{2,1,0:T(8,128)(2,1)S(1)}, u32[]{:S(2)}, u32[]{:S(2)}) async-start(bf16[32,10,128]{2,1,0:T(8,128)(2,1)} %reshape_transpose_reshape.7), calls=%async_computation.4 | async-start | bytes 262144 | tf_op jit(solution)/shard_map/all_to_all | solution.py:235
  (37 other events, 510.0 us)
Sparse Core Ops, SparseCore 0:
  83.9 59.0 all-gather.4
where the time goes:
time: 211 us; the launch traced here: 210 us
  starting transfers between devices  61.9 us (29%)
  waiting for transfers between devices  55.4 us (26%)
  blocking collectives  33.8 us (16%)
  local copies, waits for them, and re-layouts  20.5 us (10%)
  between operations  15.8 us (7%)
  other arithmetic  15.1 us (7%)
  matrix products  7.95 us (4%)
    all_gather x2, blocking collectives, entering_2(): lax.all_gather(part.astype(kind), axis)  31.3 us
    all_to_all x1, starting transfers between devices, expert_return(): returned = lax.all_to_all(back, EP, split_axis=0, concat_axis=0, tiled=True)  19.9 us
    all_gather x1, waiting for transfers between devices, entering_2(): lax.all_gather(part.astype(kind), axis)  19.8 us
    all_to_all x1, waiting for transfers between devices, expert_return(): returned = lax.all_to_all(back, EP, split_axis=0, concat_axis=0, tiled=True)  15 us
    all_to_all x1, starting transfers between devices, expert_terms(): lax.all_to_all(outgoing.reshape(experts, capacity, columns), EP, split_ax...  13.6 us
    all_to_all x2, waiting for transfers between devices, sent_and_summed(): lax.all_to_all(parts, axis, split_axis=0, concat_axis=0, tiled=True)  11.3 us
    ppermute x3, starting transfers between devices, passed_along(): return lax.ppermute(block, axis, route)  10.9 us
    all_to_all x2, starting transfers between devices, sent_and_summed(): lax.all_to_all(parts, axis, split_axis=0, concat_axis=0, tiled=True)  10.7 us
  transfers between devices with their start and end apart: 9, of which 4 were waited for; matrix products, arithmetic and copies ran while one was open for 19% of the time, Pallas kernels for 0%

commit v1 on v0

v1 whole, which is shorter than its diff:
```python
import functools

import jax
import jax.numpy as jnp
from jax import lax
from jax.experimental import pallas as pl
from jax.experimental.pallas import tpu as pltpu
from jax.sharding import Mesh
from jax.sharding import PartitionSpec as P

HEAD_DIM = 64
STATE = 128
BLOCK = 128
EP = ("ep_0", "ep_1")
SLOTS = 16
LOG_ROW = 10
VMEM = 16 << 20
F32 = jnp.float32
BF16 = jnp.bfloat16

eps = 1e-06


def iota(shape, dim):
    return lax.broadcasted_iota(jnp.int32, shape, dim)


def dot(a, b, ca=1, cb=0, precision=None):
    return lax.dot_general(
        a, b, (((ca,), (cb,)), ((), ())), precision=precision, preferred_element_type=F32
    )


def silu(x):
    return x * (1.0 / (1.0 + jnp.exp(-x)))


def softplus(x):
    return jnp.maximum(x, 0.0) + jnp.log1p(jnp.exp(-jnp.abs(x)))


def kernel_call(body, outs, args, flops, scratch=()):
    size = sum(a.size * a.dtype.itemsize for a in args)
    size += sum(o.size * o.dtype.itemsize for o in outs)
    return pl.pallas_call(
        body,
        out_shape=outs,
        in_specs=[pl.BlockSpec(memory_space=pltpu.VMEM)] * len(args),
        out_specs=[pl.BlockSpec(memory_space=pltpu.VMEM)] * len(outs),
        scratch_shapes=scratch,
        cost_estimate=pl.CostEstimate(flops=flops, bytes_accessed=size, transcendentals=0),
        compiler_params=pltpu.CompilerParams(vmem_limit_bytes=VMEM),
    )(*args)


def shape(dims, kind):
    return jax.ShapeDtypeStruct(dims, kind)


def slots_of(routing_ref):
    tokens = routing_ref.shape[0]
    expert = iota((tokens, 128), 1)
    first = expert == routing_ref[:, 0:1]
    second = expert == routing_ref[:, 1:2]
    member = jnp.where(first | second, 1.0, 0.0).astype(BF16)
    earlier = jnp.where(iota((tokens, tokens), 0) > iota((tokens, tokens), 1), 1.0, 0.0)
    place = dot(earlier.astype(BF16), member) + (expert * SLOTS).astype(F32)
    return [
        jnp.sum(jnp.where(chosen, place, 0.0), axis=1, keepdims=True).astype(jnp.int32)
        for chosen in (first, second)
    ]


def log_decay_of(step_ref, extra_ref, rate_ref):
    step = softplus(step_ref[...])
    return step, step * -jnp.exp(rate_ref[...]) + extra_ref[...]


def dispatch_body(tok_ref, gain_ref, routing_ref, step_ref, extra_ref, rate_ref, out_ref, wide):
    tokens, model = tok_ref.shape
    rows = tok_ref[...].astype(F32)
    scale = lax.rsqrt(jnp.sum(rows * rows, axis=1, keepdims=True) * (1.0 / model) + eps)
    columns = pl.ds(pl.multiple_of(lax.axis_index("tp") * 128, 128), 128)
    own = (tok_ref[:, columns].astype(F32) * scale * gain_ref[:, columns]).astype(BF16)
    slots = slots_of(routing_ref)
    total = out_ref.shape[0]
    place = iota((tokens, total), 1)
    pick = jnp.where((place == slots[0]) | (place == slots[1]), 1.0, 0.0).astype(BF16)
    sent = dot(pick, own, 0, 0)
    _, log_decay = log_decay_of(step_ref, extra_ref, rate_ref)
    heads = log_decay.shape[1]
    left = jnp.sum(log_decay, axis=0, keepdims=True)
    wide[...] = jnp.zeros_like(wide)
    for part in range(3):
        piece = left.astype(BF16).astype(F32)
        wide[part : part + 1, 0:heads] = piece
        left = left - piece
    sent = sent.reshape(total // SLOTS, SLOTS, 128)
    row = iota(sent.shape, 1)
    for part in range(3):
        sent = jnp.where(row == LOG_ROW + part, wide[part : part + 1, :][None], sent)
    out_ref[...] = sent.reshape(total, 128).astype(BF16)


def spread_body(capacity, in_ref, out_ref):
    count = out_ref.shape[1]
    row = iota((count, in_ref.shape[0]), 0)
    source = row // capacity * SLOTS + row % capacity
    pick = jnp.where(iota(source.shape, 1) == source, 1.0, 0.0).astype(BF16)
    packed = dot(pick, in_ref[...]).astype(BF16)
    for peer in range(out_ref.shape[0]):
        out_ref[peer] = packed


def ffn_body(in_ref, gate_ref, up_ref, down_ref, out_ref):
    parts, rows, width = in_ref.shape
    total = jnp.zeros((rows, 2 * width), F32)
    for k in range(0, parts, 2):
        left = jnp.concatenate([in_ref[k], in_ref[k + 1]], axis=1)
        span = pl.ds(k * width, 2 * width)
        right = jnp.concatenate([gate_ref[span, :], up_ref[span, :]], axis=1)
        total = total + dot(left, right)
    hidden = (silu(total[:, :width]) * total[:, width:]).astype(BF16)
    for k in range(0, parts, 2):
        value = dot(hidden, down_ref[:, k * width : (k + 2) * width]).astype(BF16)
        out_ref[k] = value[:, :width]
        out_ref[k + 1] = value[:, width:]


def sum_of(in_ref):
    total = in_ref[0].astype(F32)
    for k in range(1, in_ref.shape[0]):
        total = total + in_ref[k].astype(F32)
    return total.astype(BF16)


def expert_sum_body(capacity, in_ref, out_ref):
    total = sum_of(in_ref)
    count = total.shape[0]
    row = iota((out_ref.shape[0], count), 0)
    source = jnp.where(row % SLOTS < capacity, row // SLOTS * capacity + row % SLOTS, -1)
    pick = jnp.where(iota(source.shape, 1) == source, 1.0, 0.0).astype(BF16)
    out_ref[...] = dot(pick, total).astype(BF16)


def sum_body(in_ref, out_ref):
    out_ref[...] = sum_of(in_ref)


def combine_body(table_ref, routing_ref, score_ref, out_ref):
    tokens = routing_ref.shape[0]
    scores = score_ref[...]
    whole = scores[:, 0:1] + scores[:, 1:2]
    place = iota((tokens, table_ref.shape[0]), 1)
    total = jnp.zeros(out_ref.shape, F32)
    for index, slot in enumerate(slots_of(routing_ref)):
        pick = jnp.where(place == slot, 1.0, 0.0).astype(BF16)
        total = total + scores[:, index : index + 1] / whole * dot(pick, table_ref[...])
    out_ref[...] = total.astype(BF16)


def conv_silu(values_ref, prior_ref, taps_ref, start, held):
    length = values_ref.shape[0]
    reach = taps_ref.shape[0] - 1
    held[8 - reach : 8, :] = prior_ref[start : start + reach, :].astype(F32)
    held[8 : 8 + length, :] = values_ref[...].astype(F32)
    total = jnp.zeros(values_ref.shape, F32)
    for k in range(reach + 1):
        total = total + held[8 - reach + k : 8 - reach + k + length, :] * taps_ref[
            k : k + 1, :
        ].astype(F32)
    return silu(total).astype(BF16)


def running_sum(values):
    length = values.shape[0]
    reach = 1
    row = iota(values.shape, 0)
    while reach < length:
        moved = pltpu.roll(values, reach, 0)
        values = values + jnp.where(row >= reach, moved, 0.0)
        reach *= 2
    return values


def pair(left, right, dims, dim):
    return jnp.where(iota(dims, dim) < HEAD_DIM, left, right)


def block_terms(block, step_all, log_all):
    rows = slice(block * BLOCK, (block + 1) * BLOCK)
    step = step_all[rows]
    decay = running_sum(log_all[rows])
    return rows, step, decay, decay[BLOCK - 1 : BLOCK, :]


def states_body(
    x_ref, b_ref, c_ref, prior_ref, xt_ref, bt_ref, ct_ref, step_ref, extra_ref, rate_ref,
    xo_ref, bo_ref, co_ref, first_ref, total_ref, held,
):
    xo_ref[...] = conv_silu(x_ref, prior_ref, xt_ref, 0, held)
    bo_ref[...] = conv_silu(b_ref, prior_ref, bt_ref, 3, held)
    co_ref[...] = conv_silu(c_ref, prior_ref, ct_ref, 6, held)
    step_all, log_all = log_decay_of(step_ref, extra_ref, rate_ref)
    wide = (BLOCK, 128)
    for group in range(x_ref.shape[1] // 128):
        columns = slice(group * 128, (group + 1) * 128)
        a, b = 2 * group, 2 * group + 1
        state = None
        for block in range(x_ref.shape[0] // BLOCK):
            rows, step, decay, last = block_terms(block, step_all, log_all)
            x = xo_ref[rows, columns].astype(F32)
            x_step = (x * pair(step[:, a : a + 1], step[:, b : b + 1], wide, 1)).astype(BF16)
            left = jnp.exp(last - decay)
            weighted = x_step.astype(F32) * pair(left[:, a : a + 1], left[:, b : b + 1], wide, 1)
            new = dot(weighted.astype(BF16), bo_ref[rows, columns], 0, 0)
            if state is None:
                first_ref[columns, :] = new
                state = new
            else:
                kept = jnp.exp(last)
                state = state * pair(kept[:, a : a + 1], kept[:, b : b + 1], wide, 0) + new
        total_ref[columns, :] = state.astype(BF16)


def carry_body(moved_ref, table_ref, out_ref):
    sources = table_ref.shape[0] // SLOTS
    rows = moved_ref.shape[0] // sources
    me = lax.axis_index("ep_0") * 2 + lax.axis_index("ep_1")
    head = me * rows // HEAD_DIM
    sent = table_ref[...].reshape(sources, SLOTS, 128).astype(F32)
    row, lane = iota(sent.shape, 1), iota(sent.shape, 2)
    wanted = (row >= LOG_ROW) & (row < LOG_ROW + 3) & (lane == head)
    logs = jnp.sum(jnp.sum(jnp.where(wanted, sent, 0.0), axis=2, keepdims=True), axis=1)
    decay = jnp.exp(logs)
    state = jnp.zeros((rows, 128), F32)
    for k in range(sources):
        place = slice(k * rows, (k + 1) * rows)
        out_ref[place, :] = state.astype(BF16)
        state = state * decay[k : k + 1, :] + moved_ref[place, :].astype(F32)


def mixer_body(
    x_ref, b_ref, c_ref, gate_ref, first_ref, income_ref, step_ref, extra_ref, rate_ref,
    skip_ref, gain_ref, weight_ref, out_ref, normed,
):
    step_all, log_all = log_decay_of(step_ref, extra_ref, rate_ref)
    wide = (BLOCK, 128)
    causal = iota(wide, 0) >= iota(wide, 1)
    for block in range(x_ref.shape[0] // BLOCK):
        rows, step, decay, last = block_terms(block, step_all, log_all)
        grown = jnp.exp(decay)
        for group in range(x_ref.shape[1] // 128):
            columns = slice(group * 128, (group + 1) * 128)
            a, b = 2 * group, 2 * group + 1
            x = x_ref[rows, columns].astype(F32)
            x_step = (x * pair(step[:, a : a + 1], step[:, b : b + 1], wide, 1)).astype(BF16)
            c = c_ref[rows, columns]
            inner = dot(c, b_ref[rows, columns], 1, 1)
            parts = []
            for head in (a, b):
                along = jnp.broadcast_to(decay[:, head : head + 1], wide)
                distance = along - along.T
                scale = jnp.where(causal, jnp.exp(jnp.where(causal, distance, 0.0)), 0.0)
                parts.append(dot((inner * scale).astype(BF16), x_step))
            y = pair(parts[0], parts[1], wide, 1)
            entering = income_ref[columns, :].astype(F32)
            if block > 0:
                entering = entering * pair(kept[:, a : a + 1], kept[:, b : b + 1], wide, 0)
                entering = entering + first_ref[columns, :]
            off = dot(c, entering.astype(BF16), 1, 1)
            off = off * pair(grown[:, a : a + 1], grown[:, b : b + 1], wide, 1)
            skip = pair(skip_ref[:, a : a + 1], skip_ref[:, b : b + 1], wide, 1)
            mixed = (y + off + skip * x) * silu(gate_ref[rows, columns].astype(F32))
            mean = jnp.sum(mixed * mixed, axis=1, keepdims=True) * (1.0 / 128)
            mixed = mixed * lax.rsqrt(mean + eps) * gain_ref[:, columns]
            normed[rows, columns] = mixed.astype(BF16)
        kept = jnp.exp(last)
    for k in range(0, out_ref.shape[0], 2):
        value = dot(normed[...], weight_ref[:, k * 128 : (k + 2) * 128]).astype(BF16)
        out_ref[k] = value[:, :128]
        out_ref[k + 1] = value[:, 128:]


def all_to_all(value, axis):
    return lax.all_to_all(value, axis, split_axis=0, concat_axis=0, tiled=True)


def per_device(
    mixer_input_channels,
    input_state_projection,
    output_state_projection,
    output_gate_logits,
    step_size_logits,
    extra_log_decay,
    mixer_channel_taps,
    input_state_taps,
    output_state_taps,
    decay_rate_log,
    head_skip_weight,
    grouped_norm_gain,
    mixer_output_weight,
    expert_input_tokens,
    routing,
    router_chosen_scores,
    expert_norm_gain,
    expert_gate_weight,
    expert_up_weight,
    expert_down_weight,
):
    parts = lax.axis_size("tp")
    devices = lax.axis_size(EP)
    length, channels = mixer_input_channels.shape
    reach = mixer_channel_taps.shape[0] - 1
    tokens, model = expert_input_tokens.shape
    top = routing.shape[1]
    capacity = (tokens * top * 5 + 4 * devices - 1) // (4 * devices)
    slots = devices * SLOTS
    rate, skip = decay_rate_log[None], head_skip_weight[None]

    edge = jnp.concatenate(
        [
            v[length - reach :]
            for v in (mixer_input_channels, input_state_projection, output_state_projection)
        ],
        axis=0,
    )
    prior = lax.ppermute(edge, EP, [(i, i + 1) for i in range(devices - 1)])

    (outgoing,) = kernel_call(
        dispatch_body,
        [shape((slots, 128), BF16)],
        (expert_input_tokens, expert_norm_gain[None], routing, step_size_logits, extra_log_decay, rate),
        2 * slots * tokens * 128,
        [pltpu.VMEM((8, 128), F32)],
    )
    arrived = all_to_all(outgoing.reshape(devices, SLOTS, 128), EP).reshape(slots, 128)

    x_conv, b_conv, c_conv, first, total = kernel_call(
        states_body,
        [shape((length, channels), BF16)] * 3
        + [shape((channels, STATE), F32), shape((channels, STATE), BF16)],
        (
            mixer_input_channels, input_state_projection, output_state_projection, prior,
            mixer_channel_taps, input_state_taps, output_state_taps,
            step_size_logits, extra_log_decay, rate,
        ),
        2 * length * channels * STATE,
        [pltpu.VMEM((length + 8, channels), F32)],
    )
    piece = channels // devices
    moved = all_to_all(total.reshape(devices, piece, STATE), EP).reshape(channels, STATE)

    (copies,) = kernel_call(
        functools.partial(spread_body, capacity),
        [shape((parts, devices * capacity, 128), BF16)],
        (arrived,),
        2 * slots * devices * capacity * 128,
    )
    gathered = all_to_all(copies, "tp")

    (carried,) = kernel_call(
        carry_body, [shape((channels, STATE), BF16)], (moved, arrived), 4 * channels * STATE
    )
    income = all_to_all(carried.reshape(devices, piece, STATE), EP).reshape(channels, STATE)

    (partial_rows,) = kernel_call(
        ffn_body,
        [shape((parts, devices * capacity, 128), BF16)],
        (gathered, expert_gate_weight[0], expert_up_weight[0], expert_down_weight[0]),
        6 * devices * capacity * model * 128,
    )
    expert_parts = all_to_all(partial_rows, "tp")

    (mixer_part,) = kernel_call(
        mixer_body,
        [shape((parts, length, 128), BF16)],
        (
            x_conv, b_conv, c_conv, output_gate_logits, first, income,
            step_size_logits, extra_log_decay, rate, skip, grouped_norm_gain[None],
            mixer_output_weight,
        ),
        2 * length * channels * model,
        [pltpu.VMEM((length, channels), BF16)],
    )
    mixer_parts = all_to_all(mixer_part, "tp")

    (back,) = kernel_call(
        functools.partial(expert_sum_body, capacity),
        [shape((slots, 128), BF16)],
        (expert_parts,),
        2 * slots * devices * capacity * 128,
    )
    table = all_to_all(back.reshape(devices, SLOTS, 128), EP).reshape(slots, 128)

    (mixer_output_first,) = kernel_call(
        sum_body, [shape((length, 128), BF16)], (mixer_parts,), parts * length * 128
    )
    (moe_out,) = kernel_call(
        combine_body,
        [shape((tokens, 128), BF16)],
        (table, routing, router_chosen_scores),
        4 * tokens * slots * 128,
    )
    return (mixer_output_first, moe_out)


def solution(mesh):
    split = Mesh(mesh.devices.reshape(16, 2, mesh.shape["tp"]), ("ep_0", "ep_1", "tp"))
    in_specs = (
        P(EP, "tp"),
        P(EP, "tp"),
        P(EP, "tp"),
        P(EP, "tp"),
        P(EP, "tp"),
        P(EP, "tp"),
        P(None, "tp"),
        P(None, "tp"),
        P(None, "tp"),
        P("tp"),
        P("tp"),
        P("tp"),
        P("tp", None),
        P(EP, None),
        P(EP, None),
        P(EP, None),
        P(),
        P(EP, None, "tp"),
        P(EP, None, "tp"),
        P(EP, "tp", None),
    )
    out_specs = (P(EP, "tp"), P(EP, "tp"))
    return jax.shard_map(
        per_device, mesh=split, in_specs=in_specs, out_specs=out_specs, check_vma=False
    )
```

time: 211 us -> 174 us (0.82)
  waiting for transfers between devices: 55.4 us -> 90.5 us
  blocking collectives: 33.8 us -> 0 us
  other arithmetic: 15.1 us -> 0.01 us
  between operations: 15.8 us -> 0.92 us
  Pallas kernels: 0 us -> 13.7 us
  local copies, waits for them, and re-layouts: 20.5 us -> 8.12 us
  matrix products: 7.95 us -> 0 us
  starting transfers between devices: 61.9 us -> 59.4 us
    all_to_all x5 -> x7, waiting for transfers between devices: 35.6 us -> 89.8 us  [all_to_all(): return lax.all_to_all(value, axis, split_axis=0, concat_axis=0, tiled=True)]
    all_gather x2 -> x0, blocking collectives: 31.3 us -> none  [entering_2(): lax.all_gather(part.astype(kind), axis)]
    all_gather x1 -> x0, waiting for transfers between devices: 19.8 us -> none  [entering_2(): lax.all_gather(part.astype(kind), axis)]
    pallas_call x0 -> x9, Pallas kernels: none -> 13.7 us  [kernel_call(): pl.pallas_call(body, out_shape=outs, in_specs=[pl.BlockSpec(memory_space=...]
    convert_element_type x17 -> x0, other arithmetic: 8.28 us -> none  [the longest x2 2.2 us: conv_silu(): return jax.nn.silu(total).astype(jnp.bfloat16)]
    dot_general x10 -> x0, matrix products: 7.95 us -> none  [the longest x1 3.94 us: expert_terms(): jnp.einsum('erf,efd->erd', hidden, expert_down_weight, preferred_element_...]
    ppermute x3 -> x1, starting transfers between devices: 10.9 us -> 3.54 us  [per_device(): prior = lax.ppermute(edge, EP, [(i, i + 1) for i in range(devices - 1)])]
    all_to_all x5 -> x7, starting transfers between devices: 51 us -> 55.9 us  [all_to_all(): return lax.all_to_all(value, axis, split_axis=0, concat_axis=0, tiled=True)]
  transfers between devices with their start and end apart: 9 -> 8, of which waited for: 4 -> 8; matrix products, arithmetic and copies ran while one was open for 19% -> 0% of each run, Pallas kernels for 0% -> 7%
where the time goes in v1:
time: 174 us; the launch traced here: 173 us
  waiting for transfers between devices  90.5 us (52%)
  starting transfers between devices  59.4 us (34%)
  Pallas kernels  13.7 us (8%)
  local copies, waits for them, and re-layouts  8.12 us (5%)
    all_to_all x7, waiting for transfers between devices, all_to_all(): return lax.all_to_all(value, axis, split_axis=0, concat_axis=0, tiled=True)  89.8 us
    all_to_all x7, starting transfers between devices, all_to_all(): return lax.all_to_all(value, axis, split_axis=0, concat_axis=0, tiled=True)  55.9 us
    pallas_call x9, Pallas kernels, kernel_call(): pl.pallas_call(body, out_shape=outs, in_specs=[pl.BlockSpec(memory_space=...  13.7 us
    unnamed x48, local copies, waits for them, and re-layouts  7.41 us
    ppermute x1, starting transfers between devices, per_device(): prior = lax.ppermute(edge, EP, [(i, i + 1) for i in range(devices - 1)])  3.54 us
  transfers between devices with their start and end apart: 8, of which 8 were waited for; matrix products, arithmetic and copies ran while one was open for 0% of the time, Pallas kernels for 7%

profile of v1, /device:TPU:1, one launch (start us, length us, event | category | flops | bytes accessed | tf_op | source)
XLA Modules:
  0.0 172.7 jit_solution(456939867609837303)
XLA Ops:
  3.2 1.0 copy-done.1
  5.6 1.2 shard_map.204
  6.8 16.7 %all-to-all-start.1 = ((bf16[32,16,128]{2,1,0:T(8,128)(2,1)}), bf16[32,16,128]{2,1,0:T(8,128)(2,1)S(1)}, u32[]{:S(2)}, u32[]{:S(2)}) async-start(bf16[32,16,128]{2,1,0:T(8,128)(2,1)} %bitcast.4), calls=%async_computation.1 | async-start | bytes 262144 | tf_op jit(solution)/shard_map/all_to_all | solution.py:286
  24.3 3.5 %collective-permute-start = (bf16[9,256]{1,0:T(8,128)(2,1)S(1)}, bf16[9,256]{1,0:T(8,128)(2,1)S(1)}, u32[]{:S(2)}, u32[]{:S(2)}) collective-permute-start(bf16[9,256]{1,0:T(8,128)(2,1)S(1)} %pad_maximum_fusion), channel_id=1, source_target_pairs={{0,16},{16,32},{32,48},{48,64},{64,80},{80,96},{96,112},{112,128},... | collective-permute-start | bytes 13832 | tf_op jit(solution)/shard_map/ppermute | solution.py:328
  28.7 1.8 %shard_map.203 = (bf16[256,256]{1,0:T(8,128)(2,1)S(1)}, bf16[256,256]{1,0:T(8,128)(2,1)S(1)}, bf16[256,256]{1,0:T(8,128)(2,1)S(1)}, f32[256,128]{1,0:T(8,128)S(1)}, bf16[256,128]{1,0:T(8,128)(2,1)}) custom-call(bf16[256,256]{1,0:T(8,128)(2,1)S(1)} %copy-done.5, bf16[256,256]{1,0:T(8,128)(2,1)S(1)} %copy-done.6, bf16[256,256]{1,0:T(8,128)(2,1)S(1)} %copy-done.7, ...), custom_call_target="tpu_custom_call" | custom-call | flops 16777216 | bytes 1002000 | tf_op jit(solution)/shard_map/pallas_call | solution.py:45
  31.8 7.6 %all-to-all-done.1 = bf16[32,16,128]{2,1,0:T(8,128)(2,1)S(1)} async-done(((bf16[32,16,128]{2,1,0:T(8,128)(2,1)}), bf16[32,16,128]{2,1,0:T(8,128)(2,1)S(1)}, u32[]{:S(2)}, u32[]{:S(2)}) %all-to-all-start.1) | async-done | bytes 131104 | tf_op jit(solution)/shard_map/all_to_all | solution.py:286
  39.4 6.9 %all-to-all-start = ((bf16[32,8,128]{2,1,0:T(8,128)(2,1)}), bf16[32,8,128]{2,1,0:T(8,128)(2,1)S(1)}, u32[]{:S(2)}, u32[]{:S(2)}) async-start(bf16[32,8,128]{2,1,0:T(8,128)(2,1)} %bitcast.1), calls=%async_computation | async-start | bytes 131072 | tf_op jit(solution)/shard_map/all_to_all | solution.py:286
  46.2 1.4 shard_map.208
  47.6 11.6 %all-to-all-done = bf16[32,8,128]{2,1,0:T(8,128)(2,1)S(1)} async-done(((bf16[32,8,128]{2,1,0:T(8,128)(2,1)}), bf16[32,8,128]{2,1,0:T(8,128)(2,1)S(1)}, u32[]{:S(2)}, u32[]{:S(2)}) %all-to-all-start) | async-done | bytes 65568 | tf_op jit(solution)/shard_map/all_to_all | solution.py:286
  59.2 6.8 %all-to-all-start.4 = ((bf16[16,320,128]{2,1,0:T(8,128)(2,1)}), bf16[16,320,128]{2,1,0:T(8,128)(2,1)S(1)}, u32[]{:S(2)}, u32[]{:S(2)}) async-start(bf16[16,320,128]{2,1,0:T(8,128)(2,1)} %shard_map.208), calls=%async_computation.4 | async-start | bytes 2621440 | tf_op jit(solution)/shard_map/all_to_all | solution.py:286
  66.8 17.1 %all-to-all-done.4.in_ref = bf16[16,320,128]{2,1,0:T(8,128)(2,1)S(1)} async-done(((bf16[16,320,128]{2,1,0:T(8,128)(2,1)}), bf16[16,320,128]{2,1,0:T(8,128)(2,1)S(1)}, u32[]{:S(2)}, u32[]{:S(2)}) %all-to-all-start.4) | async-done | bytes 1310752 | tf_op jit(solution)/shard_map/all_to_all | solution.py:286
  83.9 7.5 %all-to-all-start.2 = ((bf16[32,8,128]{2,1,0:T(8,128)(2,1)}), bf16[32,8,128]{2,1,0:T(8,128)(2,1)S(1)}, u32[]{:S(2)}, u32[]{:S(2)}) async-start(bf16[32,8,128]{2,1,0:T(8,128)(2,1)} %bitcast.6), calls=%async_computation.2 | async-start | bytes 131072 | tf_op jit(solution)/shard_map/all_to_all | solution.py:286
  91.4 1.0 copy-done.4
  92.5 2.6 %shard_map.209 = bf16[16,320,128]{2,1,0:T(8,128)(2,1)} custom-call(bf16[16,320,128]{2,1,0:T(8,128)(2,1)S(1)} %all-to-all-done.4.in_ref, bf16[2048,128]{1,0:T(8,128)(2,1)S(1)} %bitcast.18, bf16[2048,128]{1,0:T(8,128)(2,1)S(1)} %bitcast.19, bf16[128,2048]{1,0:T(8,128)(2,1)S(1)} %bitcast.20), custom_call_target="tpu_custom_call" | custom-call | flops 503316480 | bytes 4194304 | tf_op jit(solution)/shard_map/pallas_call | solution.py:45
  95.1 9.3 %all-to-all-done.2 = bf16[32,8,128]{2,1,0:T(8,128)(2,1)S(1)} async-done(((bf16[32,8,128]{2,1,0:T(8,128)(2,1)}), bf16[32,8,128]{2,1,0:T(8,128)(2,1)S(1)}, u32[]{:S(2)}, u32[]{:S(2)}) %all-to-all-start.2) | async-done | bytes 65568 | tf_op jit(solution)/shard_map/all_to_all | solution.py:286
  104.4 3.7 %all-to-all-start.5 = ((bf16[16,320,128]{2,1,0:T(8,128)(2,1)}), bf16[16,320,128]{2,1,0:T(8,128)(2,1)S(1)}, u32[]{:S(2)}, u32[]{:S(2)}) async-start(bf16[16,320,128]{2,1,0:T(8,128)(2,1)} %shard_map.209), calls=%async_computation.5 | async-start | bytes 2621440 | tf_op jit(solution)/shard_map/all_to_all | solution.py:286
  108.2 2.9 %shard_map.206 = bf16[16,256,128]{2,1,0:T(8,128)(2,1)} custom-call(bf16[256,256]{1,0:T(8,128)(2,1)S(1)} %get-tuple-element.7.x_ref, bf16[256,256]{1,0:T(8,128)(2,1)S(1)} %get-tuple-element.8.b_ref, bf16[256,256]{1,0:T(8,128)(2,1)S(1)} %copy-done.10, bf16[256,256]{1,0:T(8,128)(2,1)S(1)} %copy-done.8, f32[256,128]{1,0:T(8,128)S(1)} %copy-done.12, ...), custom_call_target="tpu_custom_call" | custom-call | flops 268435456 | bytes 2827296 | tf_op jit(solution)/shard_map/pallas_call | solution.py:45
  111.1 15.2 %all-to-all-done.5.in_ref = bf16[16,320,128]{2,1,0:T(8,128)(2,1)S(1)} async-done(((bf16[16,320,128]{2,1,0:T(8,128)(2,1)}), bf16[16,320,128]{2,1,0:T(8,128)(2,1)S(1)}, u32[]{:S(2)}, u32[]{:S(2)}) %all-to-all-start.5) | async-done | bytes 1310752 | tf_op jit(solution)/shard_map/all_to_all | solution.py:286
  126.3 4.6 %all-to-all-start.3 = ((bf16[16,256,128]{2,1,0:T(8,128)(2,1)}), bf16[16,256,128]{2,1,0:T(8,128)(2,1)S(1)}, u32[]{:S(2)}, u32[]{:S(2)}) async-start(bf16[16,256,128]{2,1,0:T(8,128)(2,1)} %shard_map.206), calls=%async_computation.3 | async-start | bytes 2097152 | tf_op jit(solution)/shard_map/all_to_all | solution.py:286
  130.9 1.1 shard_map.210
  132.0 13.9 %all-to-all-done.3.in_ref = bf16[16,256,128]{2,1,0:T(8,128)(2,1)S(1)} async-done(((bf16[16,256,128]{2,1,0:T(8,128)(2,1)}), bf16[16,256,128]{2,1,0:T(8,128)(2,1)S(1)}, u32[]{:S(2)}, u32[]{:S(2)}) %all-to-all-start.3) | async-done | bytes 1048608 | tf_op jit(solution)/shard_map/all_to_all | solution.py:286
  145.9 9.8 %all-to-all-start.6 = ((bf16[32,16,128]{2,1,0:T(8,128)(2,1)}), bf16[32,16,128]{2,1,0:T(8,128)(2,1)S(1)}, u32[]{:S(2)}, u32[]{:S(2)}) async-start(bf16[32,16,128]{2,1,0:T(8,128)(2,1)} %bitcast.13), calls=%async_computation.6 | async-start | bytes 262144 | tf_op jit(solution)/shard_map/all_to_all | solution.py:286
  156.6 15.0 %all-to-all-done.6 = bf16[32,16,128]{2,1,0:T(8,128)(2,1)S(1)} async-done(((bf16[32,16,128]{2,1,0:T(8,128)(2,1)}), bf16[32,16,128]{2,1,0:T(8,128)(2,1)S(1)}, u32[]{:S(2)}, u32[]{:S(2)}) %all-to-all-start.6) | async-done | bytes 131104 | tf_op jit(solution)/shard_map/all_to_all | solution.py:286
  171.6 1.2 shard_map.211
  (53 shorter events, 8.4 us)
Async XLA Ops:
  0.6 28.0 %copy-start.15 = (f32[4]{0:T(128)S(1)}, f32[4]{0:T(128)}, u32[]{:S(2)}) copy-start(f32[4]{0:T(128)} %param.29) | copy-start | bytes 52
  0.6 22.9 %copy-start.6 = (bf16[256,256]{1,0:T(8,128)(2,1)S(1)}, bf16[256,256]{1,0:T(8,128)(2,1)}, u32[]{:S(2)}) copy-start(bf16[256,256]{1,0:T(8,128)(2,1)} %b_ref.1) | copy-start | bytes 393220
  0.7 23.6 %copy-start.5 = (bf16[256,256]{1,0:T(8,128)(2,1)S(1)}, bf16[256,256]{1,0:T(8,128)(2,1)}, u32[]{:S(2)}) copy-start(bf16[256,256]{1,0:T(8,128)(2,1)} %x_ref.1) | copy-start | bytes 393220
  0.7 28.0 %copy-start.16 = (bf16[4,256]{1,0:T(4,128)(2,1)S(1)}, bf16[4,256]{1,0:T(4,128)(2,1)}, u32[]{:S(2)}) copy-start(bf16[4,256]{1,0:T(4,128)(2,1)} %xt_ref.1) | copy-start | bytes 6148
  0.7 28.0 %copy-start.17 = (bf16[4,256]{1,0:T(4,128)(2,1)S(1)}, bf16[4,256]{1,0:T(4,128)(2,1)}, u32[]{:S(2)}) copy-start(bf16[4,256]{1,0:T(4,128)(2,1)} %bt_ref.1) | copy-start | bytes 6148
  0.7 28.0 %copy-start.18 = (bf16[4,256]{1,0:T(4,128)(2,1)S(1)}, bf16[4,256]{1,0:T(4,128)(2,1)}, u32[]{:S(2)}) copy-start(bf16[4,256]{1,0:T(4,128)(2,1)} %ct_ref.1) | copy-start | bytes 6148
  5.6 23.1 %copy-start.7 = (bf16[256,256]{1,0:T(8,128)(2,1)S(1)}, bf16[256,256]{1,0:T(8,128)(2,1)}, u32[]{:S(2)}) copy-start(bf16[256,256]{1,0:T(8,128)(2,1)} %c_ref.1) | copy-start | bytes 393220
  6.8 32.5 %all-to-all-start.1 = ((bf16[32,16,128]{2,1,0:T(8,128)(2,1)}), bf16[32,16,128]{2,1,0:T(8,128)(2,1)S(1)}, u32[]{:S(2)}, u32[]{:S(2)}) async-start(bf16[32,16,128]{2,1,0:T(8,128)(2,1)} %bitcast.4), calls=%async_computation.1 | async-start | bytes 262144 | tf_op jit(solution)/shard_map/all_to_all | solution.py:286
  24.3 4.3 %collective-permute-start = (bf16[9,256]{1,0:T(8,128)(2,1)S(1)}, bf16[9,256]{1,0:T(8,128)(2,1)S(1)}, u32[]{:S(2)}, u32[]{:S(2)}) collective-permute-start(bf16[9,256]{1,0:T(8,128)(2,1)S(1)} %pad_maximum_fusion), channel_id=1, source_target_pairs={{0,16},{16,32},{32,48},{48,64},{64,80},{80,96},{96,112},{112,128},... | collective-permute-start | bytes 13832 | tf_op jit(solution)/shard_map/ppermute | solution.py:328
  39.4 19.9 %all-to-all-start = ((bf16[32,8,128]{2,1,0:T(8,128)(2,1)}), bf16[32,8,128]{2,1,0:T(8,128)(2,1)S(1)}, u32[]{:S(2)}, u32[]{:S(2)}) async-start(bf16[32,8,128]{2,1,0:T(8,128)(2,1)} %bitcast.1), calls=%async_computation | async-start | bytes 131072 | tf_op jit(solution)/shard_map/all_to_all | solution.py:286
  47.6 43.8 %copy-start.2 = (bf16[1,2048,128]{2,1,0:T(8,128)(2,1)S(1)}, bf16[1,2048,128]{2,1,0:T(8,128)(2,1)}, u32[]{:S(2)}) copy-start(bf16[1,2048,128]{2,1,0:T(8,128)(2,1)} %param.37) | copy-start | bytes 1572868
  47.6 43.8 %copy-start.3 = (bf16[1,2048,128]{2,1,0:T(8,128)(2,1)S(1)}, bf16[1,2048,128]{2,1,0:T(8,128)(2,1)}, u32[]{:S(2)}) copy-start(bf16[1,2048,128]{2,1,0:T(8,128)(2,1)} %param.38) | copy-start | bytes 1572868
  59.2 24.7 %all-to-all-start.4 = ((bf16[16,320,128]{2,1,0:T(8,128)(2,1)}), bf16[16,320,128]{2,1,0:T(8,128)(2,1)S(1)}, u32[]{:S(2)}, u32[]{:S(2)}) async-start(bf16[16,320,128]{2,1,0:T(8,128)(2,1)} %shard_map.208), calls=%async_computation.4 | async-start | bytes 2621440 | tf_op jit(solution)/shard_map/all_to_all | solution.py:286
  83.9 20.5 %all-to-all-start.2 = ((bf16[32,8,128]{2,1,0:T(8,128)(2,1)}), bf16[32,8,128]{2,1,0:T(8,128)(2,1)S(1)}, u32[]{:S(2)}, u32[]{:S(2)}) async-start(bf16[32,8,128]{2,1,0:T(8,128)(2,1)} %bitcast.6), calls=%async_computation.2 | async-start | bytes 131072 | tf_op jit(solution)/shard_map/all_to_all | solution.py:286
  95.1 13.0 %copy-start = (bf16[256,2048]{1,0:T(8,128)(2,1)S(1)}, bf16[256,2048]{1,0:T(8,128)(2,1)}, u32[]{:S(2)}) copy-start(bf16[256,2048]{1,0:T(8,128)(2,1)} %weight_ref.1) | copy-start | bytes 3145732
  95.1 13.0 %copy-start.8 = (bf16[256,256]{1,0:T(8,128)(2,1)S(1)}, bf16[256,256]{1,0:T(8,128)(2,1)}, u32[]{:S(2)}) copy-start(bf16[256,256]{1,0:T(8,128)(2,1)} %gate_ref.1) | copy-start | bytes 393220
  95.1 13.0 %copy-start.10 = (bf16[256,256]{1,0:T(8,128)(2,1)S(1)}, bf16[256,256]{1,0:T(8,128)(2,1)}, u32[]{:S(2)}) copy-start(bf16[256,256]{1,0:T(8,128)(2,1)} %copy-done.9) | copy-start | bytes 393220
  95.1 13.1 %copy-start.12 = (f32[256,128]{1,0:T(8,128)S(1)}, f32[256,128]{1,0:T(8,128)}, u32[]{:S(2)}) copy-start(f32[256,128]{1,0:T(8,128)} %copy-done.11) | copy-start | bytes 393220
  95.1 13.1 %copy-start.19 = (f32[256]{0:T(256)S(1)}, f32[256]{0:T(256)}, u32[]{:S(2)}) copy-start(f32[256]{0:T(256)} %param.31) | copy-start | bytes 3076
  95.1 13.1 %copy-start.20 = (f32[4]{0:T(128)S(1)}, f32[4]{0:T(128)}, u32[]{:S(2)}) copy-start(f32[4]{0:T(128)} %param.30) | copy-start | bytes 52
  104.4 21.9 %all-to-all-start.5 = ((bf16[16,320,128]{2,1,0:T(8,128)(2,1)}), bf16[16,320,128]{2,1,0:T(8,128)(2,1)S(1)}, u32[]{:S(2)}, u32[]{:S(2)}) async-start(bf16[16,320,128]{2,1,0:T(8,128)(2,1)} %shard_map.209), calls=%async_computation.5 | async-start | bytes 2621440 | tf_op jit(solution)/shard_map/all_to_all | solution.py:286
  126.3 19.6 %all-to-all-start.3 = ((bf16[16,256,128]{2,1,0:T(8,128)(2,1)}), bf16[16,256,128]{2,1,0:T(8,128)(2,1)S(1)}, u32[]{:S(2)}, u32[]{:S(2)}) async-start(bf16[16,256,128]{2,1,0:T(8,128)(2,1)} %shard_map.206), calls=%async_computation.3 | async-start | bytes 2097152 | tf_op jit(solution)/shard_map/all_to_all | solution.py:286
  130.9 24.8 %copy-start.21 = (f32[128,2]{0,1:T(2,128)S(1)}, f32[128,2]{0,1:T(2,128)}, u32[]{:S(2)}) copy-start(f32[128,2]{0,1:T(2,128)} %param.35) | copy-start | bytes 3076
  145.9 25.7 %all-to-all-start.6 = ((bf16[32,16,128]{2,1,0:T(8,128)(2,1)}), bf16[32,16,128]{2,1,0:T(8,128)(2,1)S(1)}, u32[]{:S(2)}, u32[]{:S(2)}) async-start(bf16[32,16,128]{2,1,0:T(8,128)(2,1)} %bitcast.13), calls=%async_computation.6 | async-start | bytes 262144 | tf_op jit(solution)/shard_map/all_to_all | solution.py:286
  (6 other events, 4.7 us)
